TPU v7x, 32 devices: a whole 2x2x4 slice. The times are simulated.
32 devices in a mesh: sp: 8 (over z, x), tp: 4 (over y, core).
Axes of the slice: x: 2, y: 2, z: 4, core: 2. Of those that a mesh axis runs over, the one named last changes fastest.
Arguments:
- inputs: bfloat16 [4, 1024, 1024], P(None, 'sp'), may hold values from -6 to 6
- norm_gain: float32 [1024], replicated, may hold values from 0.1 to 1.9
- query_weight: bfloat16 [1024, 3, 8, 64], P('sp', None, 'tp'), may hold values from -0.1875 to 0.1875
- key_weight: bfloat16 [1024, 3, 8, 64], P('sp', None, 'tp'), may hold values from -0.1875 to 0.1875
- value_weight: bfloat16 [1024, 3, 8, 64], P('sp', None, 'tp'), may hold values from -0.1875 to 0.1875
- query_gain: float32 [3, 64], replicated, may hold values from 0.1 to 1.9
- key_gain: float32 [3, 64], replicated, may hold values from 0.1 to 1.9
- out_weight: bfloat16 [8, 64, 1024], P('tp', None, 'sp'), may hold values from -0.75 to 0.75
Outputs:
- mixed: bfloat16 [4, 1024, 1024], P(None, 'sp', 'tp')
All inputs are finite; a program needn't handle non-finite values.
Results may differ from a plain program's by a relative error of at most 0.02.
Values may be sent and summed in bfloat16 or wider, within the bound.
A program may use at most 64 MiB of HBM per device.

v0:
```python
import math

import jax
import jax.numpy as jnp
from jax import lax
from jax.sharding import PartitionSpec as P

SPAN_CLOSE = 32
SPREAD_CENTRAL = 4
SPAN_CENTRAL = 32
SPREAD_DISTANT = 16
SPAN_DISTANT = 16


eps = 1e-06
neg_fill = -1e30


def over_all(shard, axis, dim, absorb, state):
    everything = jax.tree.map(lambda a: lax.all_gather(a, axis, axis=dim, tiled=True), shard)
    return absorb(state, everything, jnp.int32(0))


def padded(value, sides, width, wrap):
    for axis, dim in sides:
        size, length = lax.axis_size(axis), value.shape[dim]
        up = [(i, (i + 1) % size) for i in range(size if wrap else size - 1)]
        down = [(j, i) for i, j in up]
        last = lax.slice_in_dim(value, length - width, length, axis=dim)
        initial = lax.slice_in_dim(value, 0, width, axis=dim)
        before = lax.ppermute(last, axis, up)
        after = lax.ppermute(initial, axis, down)
        value = jnp.concatenate([before, value, after], axis=dim)
    return value


def passed_along(block, axis, distance):
    devices = range(lax.axis_size(axis))
    route = [(i - distance, i) for i in devices if i - distance in devices]
    return lax.ppermute(block, axis, route)


def over_all_2(shard, axis, dim, work):
    return work(lax.all_gather(shard, axis, axis=dim, tiled=True), jnp.int32(0))


def row_norm(values, gain):
    scaled = values * lax.rsqrt(jnp.mean(values * values, axis=-1, keepdims=True) + eps)
    return scaled * gain


def band_attend(queries, keys, values, margin, dilation, half, slopes, anchor, seq_len):
    batch, count, heads, width = queries.shape
    query_rows = count // dilation
    key_rows = query_rows + 2 * half
    first = margin - half * dilation
    keys = keys[:, first : first + key_rows * dilation]
    values = values[:, first : first + key_rows * dilation]
    query_sub = queries.reshape(batch, query_rows, dilation, heads, width)
    key_sub = keys.reshape(batch, key_rows, dilation, heads, width)
    value_sub = values.reshape(batch, key_rows, dilation, heads, width)
    scores = jnp.einsum(
        "barhe,bcrhe->brhac", query_sub, key_sub, precision=lax.Precision.HIGHEST
    ) / math.sqrt(width)
    offset = jnp.arange(key_rows)[None, :] - half - jnp.arange(query_rows)[:, None]
    key_place = (
        anchor + first + dilation * jnp.arange(key_rows)[None, :] + jnp.arange(dilation)[:, None]
    )
    inside = (key_place >= 0) & (key_place < seq_len)
    allowed = (jnp.abs(offset) <= half)[None, :, :] & inside[:, None, :]
    slant = -slopes[:, None, None] * (jnp.abs(offset).astype(jnp.float32) / float(half))[None]
    scores = jnp.where(allowed[None, :, None], scores + slant[None, None], neg_fill)
    log_total = jax.nn.logsumexp(scores, axis=-1)
    weights = jnp.exp(scores - log_total[..., None])
    result = jnp.einsum("brhac,bcrhe->barhe", weights, value_sub, precision=lax.Precision.HIGHEST)
    log_total = jnp.transpose(log_total, (0, 3, 1, 2)).reshape(batch, count, heads)
    return (result.reshape(batch, count, heads, width), log_total)


def assemble(own, fetched, reach):
    before = [fetched[distance] for distance in range(reach, 0, -1)]
    after = [fetched[-distance] for distance in range(1, reach + 1)]
    return jnp.concatenate(before + [own] + after, axis=1)


def body(
    inputs, norm_gain, query_weight, key_weight, value_weight, query_gain, key_gain, out_weight
):
    batch, local_sequence_count, model_width = inputs.shape
    groups = query_weight.shape[1]
    heads_here = query_weight.shape[2]
    head_width = query_weight.shape[3]
    seq_len = local_sequence_count * lax.axis_size("sp")
    place = lax.axis_index("sp") * local_sequence_count
    flat = inputs.reshape(batch * local_sequence_count, model_width).astype(jnp.float32)
    normed = row_norm(flat, norm_gain).astype(jnp.bfloat16)
    empty = jnp.zeros((batch * local_sequence_count, groups * heads_here * head_width), jnp.float32)

    def add_rows(totals, pieces, start):
        rows = pieces[0].shape[0]
        columns = lax.dynamic_slice_in_dim(normed, start, rows, 1)
        return tuple(
            (
                total
                + jnp.dot(columns, piece.reshape(rows, -1), preferred_element_type=jnp.float32)
                for total, piece in zip(totals, pieces)
            )
        )

    projected = over_all(
        (query_weight, key_weight, value_weight), "sp", 0, add_rows, (empty, empty, empty)
    )
    layout = (batch, local_sequence_count, groups, heads_here, head_width)
    queries = projected[0].astype(jnp.bfloat16).reshape(layout)
    keys = projected[1].astype(jnp.bfloat16).reshape(layout)
    values = projected[2].astype(jnp.bfloat16).reshape(layout)
    pairs = jnp.concatenate([keys, values], axis=-1)
    total_heads = heads_here * lax.axis_size("tp")
    head_index = lax.axis_index("tp") * heads_here + jnp.arange(heads_here)
    slopes = jnp.exp2(-8.0 * (head_index + 1).astype(jnp.float32) / total_heads)
    central_extent = (
        SPREAD_CENTRAL * SPAN_CENTRAL + local_sequence_count - 1
    ) // local_sequence_count
    distant_extent = (
        SPREAD_DISTANT * SPAN_DISTANT + local_sequence_count - 1
    ) // local_sequence_count
    near_window = padded(pairs[:, :, 0], (("sp", 1),), SPAN_CLOSE, False)
    mid_fetched = {}
    far_fetched = {}
    for distance in range(1, central_extent + 1):
        for direction in (1, -1):
            mid_fetched[direction * distance] = passed_along(
                pairs[:, :, 1], "sp", direction * distance
            )
    for distance in range(1, distant_extent + 1):
        for direction in (1, -1):
            far_fetched[direction * distance] = passed_along(
                pairs[:, :, 2], "sp", direction * distance
            )
    central_span_width = assemble(pairs[:, :, 1], mid_fetched, central_extent)
    distant_span_width = assemble(pairs[:, :, 2], far_fetched, distant_extent)
    settings = (
        (near_window, SPAN_CLOSE, 1, SPAN_CLOSE),
        (central_span_width, central_extent * local_sequence_count, SPREAD_CENTRAL, SPAN_CENTRAL),
        (distant_span_width, distant_extent * local_sequence_count, SPREAD_DISTANT, SPAN_DISTANT),
    )
    results = []
    totals = []
    for group in range(3):
        window, margin, dilation, half = settings[group]
        query_group = row_norm(queries[:, :, group].astype(jnp.float32), query_gain[group])
        key_group = row_norm(window[..., :head_width].astype(jnp.float32), key_gain[group])
        value_group = window[..., head_width:].astype(jnp.float32)
        result, log_total = band_attend(
            query_group,
            key_group,
            value_group,
            margin,
            dilation,
            half,
            slopes,
            place - margin,
            seq_len,
        )
        results.append(result)
        totals.append(log_total)
    weights = jax.nn.softmax(jnp.stack(totals, 0), axis=0)
    combined = jnp.sum(weights[..., None] * jnp.stack(results, 0), axis=0)
    merged = combined.astype(jnp.bfloat16).reshape(
        batch * local_sequence_count, heads_here * head_width
    )

    def project(piece, start):
        return jnp.dot(merged, piece, preferred_element_type=jnp.float32)

    terms = over_all_2(out_weight.reshape(heads_here * head_width, -1), "sp", 1, project)
    summed = lax.psum_scatter(
        terms.astype(jnp.bfloat16), "tp", scatter_dimension=1, tiled=True
    ).astype(jnp.float32)
    return summed.astype(jnp.bfloat16).reshape(batch, local_sequence_count, -1)


def solution(mesh):
    in_specs = (
        P(None, "sp", None),
        P(),
        P("sp", None, "tp", None),
        P("sp", None, "tp", None),
        P("sp", None, "tp", None),
        P(),
        P(),
        P("tp", None, "sp"),
    )
    out_specs = P(None, "sp", "tp")
    return jax.shard_map(body, mesh=mesh, in_specs=in_specs, out_specs=out_specs, check_vma=False)
```

profile of v0, /device:TPU:17, one launch (start us, length us, event | category | flops | bytes accessed | tf_op | source)
XLA Modules:
  0.0 239.4 jit_solution(4401254442556400576)
XLA Ops:
  6.5 1.6 fusion.2
  8.2 23.3 %all_gather.13 = bf16[1024,3,2,64]{0,3,2,1:T(8,128)(2,1)S(1)} all-gather(bf16[128,3,2,64]{0,3,2,1:T(8,128)(2,1)} %param.11), channel_id=1, replica_groups=mesh['sp'=8,'tp'=4] {'sp'}, dimensions={0}, use_global_device_ids=true | all-gather | bytes 884736 | tf_op jit(solution)/shard_map/all_gather | solution.py:20
  31.5 27.8 %all_gather.14 = bf16[1024,3,2,64]{0,3,2,1:T(8,128)(2,1)S(1)} all-gather(bf16[128,3,2,64]{0,3,2,1:T(8,128)(2,1)S(1)} %copy-done.9), channel_id=1, replica_groups=mesh['sp'=8,'tp'=4] {'sp'}, dimensions={0}, use_global_device_ids=true | all-gather | bytes 884736 | tf_op jit(solution)/shard_map/all_gather | solution.py:20
  61.5 1.0 copy.116
  62.9 1.0 copy.117
  64.7 3.4 %collective-permute-start.3 = (bf16[4,128,2,128]{1,3,2,0:T(8,128)(2,1)S(1)}, bf16[4,128,2,128]{1,3,2,0:T(8,128)(2,1)}, u32[]{:S(2)}, u32[]{:S(2)}) collective-permute-start(bf16[4,128,2,128]{1,3,2,0:T(8,128)(2,1)S(1)} %get-tuple-element.12), channel_id=1, source_target_pairs={{4,0},{8,4},{12,8},{16,12},{20,16},{24,20},{28,24},{5,1},{9,5},{13... | collective-permute-start | bytes 786440 | tf_op jit(solution)/shard_map/ppermute | solution.py:40
  68.1 1.9 collective-permute-start.2
  70.0 4.6 %collective-permute-start.7 = (bf16[4,128,2,128]{1,3,2,0:T(8,128)(2,1)}, bf16[4,128,2,128]{1,3,2,0:T(8,128)(2,1)}, u32[]{:S(2)}, u32[]{:S(2)}) collective-permute-start(bf16[4,128,2,128]{1,3,2,0:T(8,128)(2,1)} %get-tuple-element.11), channel_id=1, source_target_pairs={{8,0},{12,4},{16,8},{20,12},{24,16},{28,20},{9,1},{13,5},{17,9},{2... | collective-permute-start | bytes 786440 | tf_op jit(solution)/shard_map/ppermute | solution.py:40
  75.4 1.9 collective-permute-start
  77.3 4.3 %collective-permute-start.1 = (bf16[4,32,2,128]{1,3,2,0:T(8,128)(2,1)}, bf16[4,32,2,128]{1,3,2,0:T(8,128)(2,1)S(1)}, u32[]{:S(2)}, u32[]{:S(2)}) collective-permute-start(bf16[4,32,2,128]{1,3,2,0:T(8,128)(2,1)} %get-tuple-element.16), channel_id=1, source_target_pairs={{4,0},{8,4},{12,8},{16,12},{20,16},{24,20},{28,24},{5,1},{9,5},{13... | collective-permute-start | bytes 196616 | tf_op jit(solution)/shard_map/ppermute | solution.py:32
  81.7 33.5 %all_gather.12 = bf16[1024,3,2,64]{0,3,2,1:T(8,128)(2,1)S(1)} all-gather(bf16[128,3,2,64]{0,3,2,1:T(8,128)(2,1)S(1)} %copy-done.10), channel_id=1, replica_groups=mesh['sp'=8,'tp'=4] {'sp'}, dimensions={0}, use_global_device_ids=true | all-gather | bytes 884736 | tf_op jit(solution)/shard_map/all_gather | solution.py:20
  118.0 1.1 multiply_multiply_fusion.1
  119.2 1.0 multiply_multiply_fusion
  120.2 23.0 %all_gather.15 = bf16[128,1024]{1,0:T(8,128)(2,1)} all-gather(bf16[128,128]{1,0:T(8,128)(2,1)S(1)} %bitcast.129), channel_id=1, replica_groups=mesh['sp'=8,'tp'=4] {'sp'}, dimensions={1}, use_global_device_ids=true | all-gather | bytes 294912 | tf_op jit(solution)/shard_map/all_gather | solution.py:44
  143.2 2.4 %collective-permute-start.6 = (bf16[4,128,2,128]{1,3,2,0:T(8,128)(2,1)}, bf16[4,128,2,128]{1,3,2,0:T(8,128)(2,1)S(1)}, u32[]{:S(2)}, u32[]{:S(2)}) collective-permute-start(bf16[4,128,2,128]{1,3,2,0:T(8,128)(2,1)} %get-tuple-element.11), channel_id=1, source_target_pairs={{4,0},{8,4},{12,8},{16,12},{20,16},{24,20},{28,24},{5,1},{9,5},{13... | collective-permute-start | bytes 786440 | tf_op jit(solution)/shard_map/ppermute | solution.py:40
  145.6 2.9 %collective-permute-start.5 = (bf16[4,128,2,128]{1,3,2,0:T(8,128)(2,1)}, bf16[4,128,2,128]{1,3,2,0:T(8,128)(2,1)}, u32[]{:S(2)}, u32[]{:S(2)}) collective-permute-start(bf16[4,128,2,128]{1,3,2,0:T(8,128)(2,1)} %get-tuple-element.11), channel_id=1, source_target_pairs={{0,4},{4,8},{8,12},{12,16},{16,20},{20,24},{24,28},{1,5},{5,9},{9,... | collective-permute-start | bytes 786440 | tf_op jit(solution)/shard_map/ppermute | solution.py:40
  148.9 1.5 fusion.92
  150.6 1.4 convolution_bitcast_fusion.1
  152.0 4.6 %collective-permute-start.4 = (bf16[4,128,2,128]{1,3,2,0:T(8,128)(2,1)}, bf16[4,128,2,128]{1,3,2,0:T(8,128)(2,1)}, u32[]{:S(2)}, u32[]{:S(2)}) collective-permute-start(bf16[4,128,2,128]{1,3,2,0:T(8,128)(2,1)} %get-tuple-element.11), channel_id=1, source_target_pairs={{0,8},{4,12},{8,16},{12,20},{16,24},{20,28},{1,9},{5,13},{9,17},{1... | collective-permute-start | bytes 786440 | tf_op jit(solution)/shard_map/ppermute | solution.py:40
  156.7 1.1 pad_maximum_fusion
  158.5 3.7 %fusion.91 = (f32[4,4,2,32]{3,2,1,0:T(2,128)S(1)}, f32[4,4,2,32,96]{4,3,2,1,0:T(8,128)S(1)}) fusion(f32[2,32,96]{2,1,0:T(8,128)S(1)} %broadcast_multiply_fusion.1, f32[4,96,4,2,64]{4,2,1,3,0:T(4,128)S(1)} %bitcast.113, f32[4,32,4,2,64]{4,2,1,3,0:T(4,128)} %multiply_multiply_fusion.1, pred[4,32,96]{2,1,0:T(8,128)(4,1)S(1)} %broadcast_and_fusion.1), kind=kOutput, calls=%fused_computation.159 | convolution fusion | flops 75889664 | bytes 1482752 | tf_op jit(solution)/shard_map/barhe,bcrhe->brhac/dot_general | solution.py:62
  162.3 1.2 constant_dynamic-update-slice_fusion.4
  163.9 1.0 constant_dynamic-update-slice_fusion.3
  164.9 1.0 constant_dynamic-update-slice_fusion.2
  166.5 1.0 constant_dynamic-update-slice_fusion
  167.7 1.2 fusion.8
  169.0 1.9 copy.132
  170.9 6.9 %fusion.90 = (f32[4,16,2,8]{3,2,1,0:T(2,128)S(1)}, f32[4,16,2,8,40]{4,3,2,1,0:T(8,128)}) fusion(f32[2,8,40]{2,1,0:T(8,128)S(1)} %broadcast_multiply_fusion.2, f32[4,40,16,2,64]{4,2,1,3,0:T(8,128)S(1)} %bitcast.112, f32[4,8,16,2,64]{4,2,1,3,0:T(8,128)} %multiply_multiply_fusion, pred[16,8,40]{2,1,0:T(8,128)(4,1)S(1)} %broadcast_and_fusion), kind=kOutput, calls=%fused_computation.158 | convolution fusion | flops 31620096 | bytes 1748480 | tf_op jit(solution)/shard_map/barhe,bcrhe->brhac/dot_general | solution.py:62
  178.0 1.5 exponential_reduce_fusion.1
  182.5 1.2 fusion.13
  184.9 1.4 convolution_convert_fusion
  186.4 46.2 %reduce-scatter.2.cloned.1.call-done = bf16[512,256]{1,0:T(8,128)(2,1)} async-done(((bf16[512,1024]{1,0:T(8,128)(2,1)}), bf16[512,256]{1,0:T(8,128)(2,1)}) %reduce-scatter.2.cloned.1.call-update) | async-done | bytes 262160 | tf_op jit(solution)/shard_map/reduce_scatter | solution.py:177
  (131 shorter events, 13.6 us)
Async XLA Ops:
  6.5 52.8 %copy-start.3 = (bf16[4,128,1024]{2,1,0:T(8,128)(2,1)S(1)}, bf16[4,128,1024]{2,1,0:T(8,128)(2,1)}, u32[]{:S(2)}) copy-start(bf16[4,128,1024]{2,1,0:T(8,128)(2,1)} %param.8) | copy-start | bytes 3145732
  6.5 24.9 %copy-start.9 = (bf16[128,3,2,64]{0,3,2,1:T(8,128)(2,1)S(1)}, bf16[128,3,2,64]{0,3,2,1:T(8,128)(2,1)}, u32[]{:S(2)}) copy-start(bf16[128,3,2,64]{0,3,2,1:T(8,128)(2,1)} %param.12) | copy-start | bytes 294916
  6.5 52.7 %copy-start.12 = (f32[1024]{0:T(1024)S(1)}, f32[1024]{0:T(1024)}, u32[]{:S(2)}) copy-start(f32[1024]{0:T(1024)} %param.9) | copy-start | bytes 12292
  6.5 226.0 %reduce-scatter.2.cloned.1.call-start = ((), (), s32[]{:S(2)}) async-start(), calls=%async_computation.1 | async-start | bytes 1310720 | tf_op jit(solution)/shard_map/reduce_scatter | solution.py:177
  63.9 17.8 %copy-start.10 = (bf16[128,3,2,64]{0,3,2,1:T(8,128)(2,1)S(1)}, bf16[128,3,2,64]{0,3,2,1:T(8,128)(2,1)}, u32[]{:S(2)}) copy-start(bf16[128,3,2,64]{0,3,2,1:T(8,128)(2,1)} %param.10) | copy-start | bytes 294916
  64.7 51.2 %copy-start.7 = (bf16[4,128,2,128]{1,3,2,0:T(8,128)(2,1)}, bf16[4,128,2,128]{1,3,2,0:T(8,128)(2,1)S(1)}, u32[]{:S(2)}) copy-start(bf16[4,128,2,128]{1,3,2,0:T(8,128)(2,1)S(1)} %get-tuple-element.12) | copy-start | bytes 786436
  64.7 87.3 %collective-permute-start.3 = (bf16[4,128,2,128]{1,3,2,0:T(8,128)(2,1)S(1)}, bf16[4,128,2,128]{1,3,2,0:T(8,128)(2,1)}, u32[]{:S(2)}, u32[]{:S(2)}) collective-permute-start(bf16[4,128,2,128]{1,3,2,0:T(8,128)(2,1)S(1)} %get-tuple-element.12), channel_id=1, source_target_pairs={{4,0},{8,4},{12,8},{16,12},{20,16},{24,20},{28,24},{5,1},{9,5},{13... | collective-permute-start | bytes 786440 | tf_op jit(solution)/shard_map/ppermute | solution.py:40
  68.1 88.6 %collective-permute-start.2 = (bf16[4,128,2,128]{1,3,2,0:T(8,128)(2,1)S(1)}, bf16[4,128,2,128]{1,3,2,0:T(8,128)(2,1)}, u32[]{:S(2)}, u32[]{:S(2)}) collective-permute-start(bf16[4,128,2,128]{1,3,2,0:T(8,128)(2,1)S(1)} %get-tuple-element.12), channel_id=1, source_target_pairs={{0,4},{4,8},{8,12},{12,16},{16,20},{20,24},{24,28},{1,5},{5,9},{9,... | collective-permute-start | bytes 786440 | tf_op jit(solution)/shard_map/ppermute | solution.py:40
  70.0 96.5 %collective-permute-start.7 = (bf16[4,128,2,128]{1,3,2,0:T(8,128)(2,1)}, bf16[4,128,2,128]{1,3,2,0:T(8,128)(2,1)}, u32[]{:S(2)}, u32[]{:S(2)}) collective-permute-start(bf16[4,128,2,128]{1,3,2,0:T(8,128)(2,1)} %get-tuple-element.11), channel_id=1, source_target_pairs={{8,0},{12,4},{16,8},{20,12},{24,16},{28,20},{9,1},{13,5},{17,9},{2... | collective-permute-start | bytes 786440 | tf_op jit(solution)/shard_map/ppermute | solution.py:40
  75.4 67.7 %collective-permute-start = (bf16[4,32,2,128]{1,3,2,0:T(8,128)(2,1)}, bf16[4,32,2,128]{1,3,2,0:T(8,128)(2,1)S(1)}, u32[]{:S(2)}, u32[]{:S(2)}) collective-permute-start(bf16[4,32,2,128]{1,3,2,0:T(8,128)(2,1)} %get-tuple-element.15), channel_id=1, source_target_pairs={{0,4},{4,8},{8,12},{12,16},{16,20},{20,24},{24,28},{1,5},{5,9},{9,... | collective-permute-start | bytes 196616 | tf_op jit(solution)/shard_map/ppermute | solution.py:31
  77.3 68.2 %collective-permute-start.1 = (bf16[4,32,2,128]{1,3,2,0:T(8,128)(2,1)}, bf16[4,32,2,128]{1,3,2,0:T(8,128)(2,1)S(1)}, u32[]{:S(2)}, u32[]{:S(2)}) collective-permute-start(bf16[4,32,2,128]{1,3,2,0:T(8,128)(2,1)} %get-tuple-element.16), channel_id=1, source_target_pairs={{4,0},{8,4},{12,8},{16,12},{20,16},{24,20},{28,24},{5,1},{9,5},{13... | collective-permute-start | bytes 196616 | tf_op jit(solution)/shard_map/ppermute | solution.py:32
  115.9 0.7 copy-start.13
  115.9 0.7 copy-start.14
  117.9 2.3 copy-start.11
  143.2 22.8 %collective-permute-start.6 = (bf16[4,128,2,128]{1,3,2,0:T(8,128)(2,1)}, bf16[4,128,2,128]{1,3,2,0:T(8,128)(2,1)S(1)}, u32[]{:S(2)}, u32[]{:S(2)}) collective-permute-start(bf16[4,128,2,128]{1,3,2,0:T(8,128)(2,1)} %get-tuple-element.11), channel_id=1, source_target_pairs={{4,0},{8,4},{12,8},{16,12},{20,16},{24,20},{28,24},{5,1},{9,5},{13... | collective-permute-start | bytes 786440 | tf_op jit(solution)/shard_map/ppermute | solution.py:40
  145.6 18.3 %collective-permute-start.5 = (bf16[4,128,2,128]{1,3,2,0:T(8,128)(2,1)}, bf16[4,128,2,128]{1,3,2,0:T(8,128)(2,1)}, u32[]{:S(2)}, u32[]{:S(2)}) collective-permute-start(bf16[4,128,2,128]{1,3,2,0:T(8,128)(2,1)} %get-tuple-element.11), channel_id=1, source_target_pairs={{0,4},{4,8},{8,12},{12,16},{16,20},{20,24},{24,28},{1,5},{5,9},{9,... | collective-permute-start | bytes 786440 | tf_op jit(solution)/shard_map/ppermute | solution.py:40
  150.4 6.2 %copy-start.8 = (bf16[4,128,2,128]{1,3,2,0:T(8,128)(2,1)S(1)}, bf16[4,128,2,128]{1,3,2,0:T(8,128)(2,1)}, u32[]{:S(2)}) copy-start(bf16[4,128,2,128]{1,3,2,0:T(8,128)(2,1)} %copy-done.7) | copy-start | bytes 786436
  152.0 10.3 %collective-permute-start.4 = (bf16[4,128,2,128]{1,3,2,0:T(8,128)(2,1)}, bf16[4,128,2,128]{1,3,2,0:T(8,128)(2,1)}, u32[]{:S(2)}, u32[]{:S(2)}) collective-permute-start(bf16[4,128,2,128]{1,3,2,0:T(8,128)(2,1)} %get-tuple-element.11), channel_id=1, source_target_pairs={{0,8},{4,12},{8,16},{12,20},{16,24},{20,28},{1,9},{5,13},{9,17},{1... | collective-permute-start | bytes 786440 | tf_op jit(solution)/shard_map/ppermute | solution.py:40
  157.8 8.2 %copy-start = (bf16[4,384,2,128]{1,3,2,0:T(8,128)(2,1)}, bf16[4,384,2,128]{1,3,2,0:T(8,128)(2,1)S(1)}, u32[]{:S(2)}) copy-start(bf16[4,384,2,128]{1,3,2,0:T(8,128)(2,1)S(1)} %pad_maximum_fusion) | copy-start | bytes 2359300
  162.2 3.8 %copy-start.1 = (f32[4,4,2,32,96]{4,3,2,1,0:T(8,128)}, f32[4,4,2,32,96]{4,3,2,1,0:T(8,128)S(1)}, u32[]{:S(2)}) copy-start(f32[4,4,2,32,96]{4,3,2,1,0:T(8,128)S(1)} %get-tuple-element.26) | copy-start | bytes 1179652
  177.8 2.0 slice-start
  177.8 2.4 %copy-start.2 = (f32[4,4,2,32,96]{4,3,2,1,0:T(8,128)S(1)}, f32[4,4,2,32,96]{4,3,2,1,0:T(8,128)}, u32[]{:S(2)}) copy-start(f32[4,4,2,32,96]{4,3,2,1,0:T(8,128)} %copy-done.1) | copy-start | bytes 1179652
  181.4 1.1 copy-start.4
  183.7 1.0 copy-start.5
  183.7 1.1 copy-start.6
Sparse Core Ops, SparseCore 0:
  186.5 46.0 reduce-scatter.1
where the time goes:
time: 242 us; the launch traced here: 239 us
  blocking collectives  108 us (45%)
  waiting for transfers between devices  46.2 us (19%)
  starting transfers between devices  25.9 us (11%)
  matrix products  19.2 us (8%)
  local copies, waits for them, and re-layouts  14.9 us (6%)
  between operations  14.3 us (6%)
  other arithmetic  11.3 us (5%)
    all_gather x3, blocking collectives, over_all(): lax.all_gather(a, axis, axis=dim, tiled=True)  84.6 us
    reduce_scatter x1, waiting for transfers between devices, body(): lax.psum_scatter(terms.astype(jnp.bfloat16), 'tp', scatter_dimension=1, t...  46.2 us
    all_gather x1, blocking collectives, over_all_2(): return work(lax.all_gather(shard, axis, axis=dim, tiled=True), jnp.int32(0))  23 us
    ppermute x6, starting transfers between devices, passed_along(): return lax.ppermute(block, axis, route)  19.7 us
    dot_general x3, matrix products, band_attend(): jnp.einsum('barhe,bcrhe->brhac', query_sub, key_sub, precision=lax.Precis...  12.1 us
  transfers between devices with their start and end apart: 9, of which 1 were waited for; matrix products, arithmetic and copies ran while one was open for 8% of the time, Pallas kernels for 0%

commit v1 on v0

v1 whole, which is shorter than its diff:
```python
import functools
import math

import jax
import jax.numpy as jnp
from jax import lax
from jax.experimental import pallas as pl
from jax.experimental.pallas import tpu as pltpu
from jax.sharding import PartitionSpec as P

GAPS = ((1, 32), (4, 32), (16, 16))
EPS = 1e-06
NEG = -1e30
MESH = pl.DeviceIdType.MESH


def halo_plan(length):
    plan = []
    for group, (dilation, half) in enumerate(GAPS):
        reach = dilation * half
        for distance in range(1, -(-reach // length) + 1):
            plan.append((group, distance, min(length, reach - (distance - 1) * length)))
    return sorted(plan, key=lambda item: item[1])


def layer_kernel(
    n, tp, batch, length, heads, width, x_ref, gain_ref, wa_ref, wb_ref, qg_ref, kg_ref, slope_ref, out_ref,
    abuf, bbuf, win0, win1, win2, qn, bias, merged, parts, got,
    rs_send, rs_recv, ring_send, ring_recv, halo_send, halo_recv,
):
    me = lax.axis_index("sp")
    mine = lax.axis_index("tp")
    groups = len(GAPS)
    lanes = heads * width
    rows = batch * length
    half_n = n // 2

    def ring_to_sp(p):
        return jnp.where(p < half_n, 2 * p, 2 * (n - 1 - p) + 1)

    place = jnp.where(me % 2 == 0, me // 2, n - 1 - me // 2)
    forward = ring_to_sp((place + 1) % n)
    backward = ring_to_sp((place + n - 1) % n)
    bufs = (abuf, bbuf)
    firsts = (wa_ref, wb_ref)

    def hop(chunk, way, step):
        owner = ring_to_sp((place + (n - (step - 1) if way == 0 else step - 1)) % n)
        buf = bufs[chunk]
        columns = buf.shape[2]
        cut = pl.ds(0, columns)
        if step == half_n and n % 2 == 0:
            middle = (columns // 2 + 127) // 128 * 128
            cut = pl.ds(0, middle) if way == 0 else pl.ds(middle, columns - middle)
        src = firsts[chunk].at[:, cut] if step == 1 else buf.at[owner, :, cut]
        return pltpu.make_async_remote_copy(
            src_ref=src,
            dst_ref=buf.at[owner, :, cut],
            send_sem=ring_send.at[chunk, way, step - 1],
            recv_sem=ring_recv.at[chunk, way, step - 1],
            device_id={"sp": forward if way == 0 else backward},
            device_id_type=MESH,
        )

    for chunk in range(2):
        for way in range(2):
            hop(chunk, way, 1).start()
    for chunk in range(2):
        bufs[chunk][me] = firsts[chunk][...]

    flat = x_ref[...].reshape(rows, -1).astype(jnp.float32)
    scale = lax.rsqrt(jnp.mean(flat * flat, axis=-1, keepdims=True) + EPS)
    normed = (flat * scale * gain_ref[...]).astype(jnp.bfloat16)

    widths = [length + 2 * d * h for d, h in GAPS]
    starts = [sum(widths[:g]) for g in range(groups)]
    for group, (dilation, half) in enumerate(GAPS):
        reach = dilation * half
        shape = (length, widths[group])
        key = lax.broadcasted_iota(jnp.int32, shape, 1) - reach
        offset = jnp.abs(key - lax.broadcasted_iota(jnp.int32, shape, 0))
        at = key + me * length
        allowed = (offset <= reach) & (at >= 0) & (at < n * length) & ((offset & (dilation - 1)) == 0)
        distance = offset.astype(jnp.float32) / float(reach)
        for head in range(heads):
            value = jnp.where(allowed, -slope_ref[head : head + 1, :1] * distance, NEG)
            bias[head, :, starts[group] : starts[group] + widths[group]] = value

    wins = (win0, win1, win2)
    plan = halo_plan(length)
    for group, distance, count in plan:
        reach = GAPS[group][0] * GAPS[group][1]
        low = reach - (distance - 1) * length - count
        high = reach + distance * length
        blank = jnp.zeros((batch, count, 2 * lanes), jnp.bfloat16)

        @pl.when(me < distance)
        def _(group=group, low=low, count=count, blank=blank):
            wins[group][:, low : low + count, :] = blank

        @pl.when(me + distance >= n)
        def _(group=group, high=high, count=count, blank=blank):
            wins[group][:, high : high + count, :] = blank

    def finish_ring(chunk):
        for way in range(2):
            hop(chunk, way, half_n).wait_recv()

    for step in range(2, half_n + 1):
        for chunk in range(2):
            for way in range(2):
                hop(chunk, way, step - 1).wait_recv()
                hop(chunk, way, step).start()

    row_head = lax.broadcasted_iota(jnp.int32, (lanes, lanes), 0) // width
    column_head = lax.broadcasted_iota(jnp.int32, (lanes, lanes), 1) // width
    same_head = jnp.where(row_head == column_head, 1.0 / width, 0.0)

    def head_norm(block, gain):
        values = block.astype(jnp.bfloat16).astype(jnp.float32)
        mean = jnp.dot(
            values * values, same_head, precision=lax.Precision.HIGHEST, preferred_element_type=jnp.float32
        )
        return values * lax.rsqrt(mean + EPS) * gain

    finish_ring(0)
    depth = abuf.shape[0] * abuf.shape[1]
    key_values = jnp.dot(normed, abuf[...].reshape(depth, -1), preferred_element_type=jnp.float32)
    for group, (dilation, half) in enumerate(GAPS):
        reach = dilation * half
        low = 2 * lanes * group
        keys = head_norm(key_values[:, low : low + lanes], kg_ref[group : group + 1, :])
        values = key_values[:, low + lanes : low + 2 * lanes]
        wins[group][:, reach : reach + length, :lanes] = keys.astype(jnp.bfloat16).reshape(batch, length, lanes)
        wins[group][:, reach : reach + length, lanes:] = values.astype(jnp.bfloat16).reshape(batch, length, lanes)

    def halo(index, up):
        group, distance, count = plan[index]
        reach = GAPS[group][0] * GAPS[group][1]
        win = wins[group]
        if up:
            src = win.at[:, pl.ds(reach + length - count, count), :]
            dst = win.at[:, pl.ds(reach - (distance - 1) * length - count, count), :]
            target = (me + distance) % n
        else:
            src = win.at[:, pl.ds(reach, count), :]
            dst = win.at[:, pl.ds(reach + distance * length, count), :]
            target = (me + n - distance) % n
        side = 0 if up else 1
        return pltpu.make_async_remote_copy(
            src_ref=src,
            dst_ref=dst,
            send_sem=halo_send.at[side, index],
            recv_sem=halo_recv.at[side, index],
            device_id={"sp": target},
            device_id_type=MESH,
        )

    def each_halo(method_up, method_down, inward):
        for index, (group, distance, count) in enumerate(plan):
            above = me + distance < n
            below = me >= distance

            @pl.when(below if inward else above)
            def _(index=index):
                method_up(halo(index, True))

            @pl.when(above if inward else below)
            def _(index=index):
                method_down(halo(index, False))

    each_halo(lambda c: c.start(), lambda c: c.start(), False)

    finish_ring(1)
    factor = 1.0 / math.sqrt(width)
    weights = bbuf[:, :, : groups * lanes].reshape(depth, groups * lanes)
    queries = jnp.dot(normed, weights, preferred_element_type=jnp.float32)
    for group in range(groups):
        block = head_norm(queries[:, lanes * group : lanes * (group + 1)], qg_ref[group : group + 1, :] * factor)
        qn[group] = block.astype(jnp.bfloat16).reshape(batch, length, lanes)

    each_halo(lambda c: c.wait_recv(), lambda c: c.wait_recv(), True)

    lane_head = lax.broadcasted_iota(jnp.int32, (length, lanes), 1) // width

    def attend(b, carry):
        result = jnp.zeros((length, lanes), jnp.float32)
        for head in range(heads):
            here = lane_head == head
            total = jnp.zeros((length, 1), jnp.float32)
            summed = jnp.zeros((length, lanes), jnp.float32)
            for group in range(groups):
                query = qn[group, b]
                query = jnp.where(here, query, jnp.zeros_like(query))
                scores = lax.dot_general(
                    query, wins[group][b, :, :lanes], (((1,), (1,)), ((), ())), preferred_element_type=jnp.float32
                )
                scores = scores + bias[head, :, starts[group] : starts[group] + widths[group]]
                grown = jnp.exp(scores)
                total = total + jnp.sum(grown, axis=-1, keepdims=True)
                summed = summed + jnp.dot(
                    grown.astype(jnp.bfloat16), wins[group][b, :, lanes:], preferred_element_type=jnp.float32
                )
            result = jnp.where(here, summed / total, result)
        merged[b] = result.astype(jnp.bfloat16)
        return carry

    lax.fori_loop(0, batch, attend, 0)

    both = merged[...].reshape(rows, lanes)
    outs = bbuf[:, :, groups * lanes :].reshape(depth, lanes)
    span = depth // tp
    for block in range(tp):
        term = lax.dot_general(
            both, outs[block * span : (block + 1) * span], (((1,), (1,)), ((), ())), preferred_element_type=jnp.float32
        )
        parts[block] = term.astype(jnp.bfloat16)

    def exchange(shift):
        target = (mine + shift) % tp
        return pltpu.make_async_remote_copy(
            src_ref=parts.at[target],
            dst_ref=got.at[shift - 1],
            send_sem=rs_send.at[shift - 1],
            recv_sem=rs_recv.at[shift - 1],
            device_id={"tp": target},
            device_id_type=MESH,
        )

    for shift in range(1, tp):
        exchange(shift).start()
    summed = parts[mine].astype(jnp.float32)
    for shift in range(1, tp):
        exchange(shift).wait_recv()
        summed = summed + got[shift - 1].astype(jnp.float32)
    out_ref[...] = summed.astype(jnp.bfloat16).reshape(batch, length, span)

    for shift in range(1, tp):
        exchange(shift).wait_send()
    for step in range(1, half_n + 1):
        for chunk in range(2):
            for way in range(2):
                hop(chunk, way, step).wait_send()
    each_halo(lambda c: c.wait_send(), lambda c: c.wait_send(), False)


def body(n, tp, inputs, norm_gain, query_weight, key_weight, value_weight, query_gain, key_gain, out_weight):
    batch, length, model = inputs.shape
    share, groups, heads, width = query_weight.shape
    lanes = heads * width
    key_values = jnp.stack(
        [key_weight.reshape(share, groups, lanes), value_weight.reshape(share, groups, lanes)], axis=2
    ).reshape(share, groups * 2 * lanes)
    outs = out_weight.reshape(lanes, -1).T
    rest = jnp.concatenate([query_weight.reshape(share, groups * lanes), outs], axis=1)
    index = lax.axis_index("tp") * heads + jnp.arange(heads)
    slopes = jnp.exp2(-8.0 * (index + 1).astype(jnp.float32) / (heads * tp))
    slopes = jnp.broadcast_to(slopes[:, None], (heads, 128))
    total = sum(length + 2 * d * h for d, h in GAPS)
    windows = [pltpu.VMEM((batch, length + 2 * d * h, 2 * lanes), jnp.bfloat16) for d, h in GAPS]
    plan = halo_plan(length)
    vmem = pl.BlockSpec(memory_space=pltpu.VMEM)
    span = model // tp
    return pl.pallas_call(
        functools.partial(layer_kernel, n, tp, batch, length, heads, width),
        out_shape=jax.ShapeDtypeStruct((batch, length, span), jnp.bfloat16),
        in_specs=[vmem] * 7,
        out_specs=vmem,
        scratch_shapes=[
            pltpu.VMEM((n, share, key_values.shape[1]), jnp.bfloat16),
            pltpu.VMEM((n, share, rest.shape[1]), jnp.bfloat16),
            *windows,
            pltpu.VMEM((groups, batch, length, lanes), jnp.bfloat16),
            pltpu.VMEM((heads, length, total), jnp.float32),
            pltpu.VMEM((batch, length, lanes), jnp.bfloat16),
            pltpu.VMEM((tp, batch * length, span), jnp.bfloat16),
            pltpu.VMEM((tp - 1, batch * length, span), jnp.bfloat16),
            pltpu.SemaphoreType.DMA((tp - 1,)),
            pltpu.SemaphoreType.DMA((tp - 1,)),
            pltpu.SemaphoreType.DMA((2, 2, n // 2)),
            pltpu.SemaphoreType.DMA((2, 2, n // 2)),
            pltpu.SemaphoreType.DMA((2, len(plan))),
            pltpu.SemaphoreType.DMA((2, len(plan))),
        ],
        compiler_params=pltpu.CompilerParams(has_side_effects=True, vmem_limit_bytes=60 * 1024 * 1024),
        name="layer",
    )(
        inputs,
        norm_gain.reshape(1, model),
        key_values,
        rest,
        jnp.tile(query_gain, (1, heads)),
        jnp.tile(key_gain, (1, heads)),
        slopes,
    )


def solution(mesh):
    in_specs = (
        P(None, "sp", None),
        P(),
        P("sp", None, "tp", None),
        P("sp", None, "tp", None),
        P("sp", None, "tp", None),
        P(),
        P(),
        P("tp", None, "sp"),
    )
    out_specs = P(None, "sp", "tp")
    run = functools.partial(body, mesh.shape["sp"], mesh.shape["tp"])
    return jax.shard_map(run, mesh=mesh, in_specs=in_specs, out_specs=out_specs, check_vma=False)
```

time: 242 us -> 88.4 us (0.37)
  blocking collectives: 108 us -> 0 us
  Pallas kernels: 0 us -> 80.2 us
  waiting for transfers between devices: 46.2 us -> 0 us
  starting transfers between devices: 25.9 us -> 0 us
  matrix products: 19.2 us -> 0 us
  between operations: 14.3 us -> 0.07 us
  other arithmetic: 11.3 us -> 1.12 us
  local copies, waits for them, and re-layouts: 14.9 us -> 6.66 us
    all_gather x4 -> x0, blocking collectives: 108 us -> none  [the longest x3 84.6 us: over_all(): lax.all_gather(a, axis, axis=dim, tiled=True)]
    pallas_call x0 -> x1, Pallas kernels: none -> 80.2 us  [body(): pl.pallas_call(functools.partial(layer_kernel, n, tp, batch, length, head...]
    reduce_scatter x1 -> x0, waiting for transfers between devices: 46.2 us -> none  [body(): lax.psum_scatter(terms.astype(jnp.bfloat16), 'tp', scatter_dimension=1, t...]
    ppermute x8 -> x0, starting transfers between devices: 25.9 us -> none  [the longest x6 19.7 us: passed_along(): return lax.ppermute(block, axis, route)]
    dot_general x10 -> x0, matrix products: 19.2 us -> none  [the longest x3 12.1 us: band_attend(): jnp.einsum('barhe,bcrhe->brhac', query_sub, key_sub, precision=lax.Precis...]
    reduce_sum x10 -> x0, other arithmetic: 4.34 us -> none  [the longest x5 2.19 us: row_norm(): jnp.mean(values * values, axis=-1, keepdims=True) + eps]
    mul x7 -> x0, other arithmetic: 3.72 us -> none  [the longest x4 3.49 us: row_norm(): return scaled * gain]
  transfers between devices with their start and end apart: 9 -> 0, of which waited for: 1 -> 0; matrix products, arithmetic and copies ran while one was open for 8% -> 0% of each run, Pallas kernels for 0% -> 0%
where the time goes in v1:
time: 88.4 us; the launch traced here: 88.1 us
  Pallas kernels  80.2 us (91%)
  local copies, waits for them, and re-layouts  6.66 us (8%)
  other arithmetic  1.12 us (1%)
    pallas_call x1, Pallas kernels, body(): pl.pallas_call(functools.partial(layer_kernel, n, tp, batch, length, head...  80.2 us
    unnamed x11, local copies, waits for them, and re-layouts  2.47 us

profile of v1, /device:TPU:17, one launch (start us, length us, event | category | flops | bytes accessed | tf_op | source)
XLA Modules:
  0.0 88.1 jit_solution(7000131201622501738)
XLA Ops:
  0.0 0.0 copy-start.1
  0.0 1.1 %copy.13 = bf16[128,3,1,128]{3,2,1,0:T(2,128)(2,1)S(1)} copy(bf16[128,3,1,128]{0,3,1,2:T(8,128)(2,1)} %bitcast.8) | data formatting | bytes 196608 | tf_op jit(solution)/shard_map/stack;reshape | solution.py:251
  1.1 0.0 copy-done.1
  1.1 0.2 copy.14
  1.3 0.5 pad_maximum_fusion
  1.7 0.0 copy-start
  1.7 0.8 reshape.29.wa_ref
  2.5 0.1 copy-done
  2.6 0.0 copy-start.2
  2.6 0.1 copy.16
  2.7 0.6 copy-done.2
  3.4 0.1 copy.15
  3.5 0.0 copy-start.3
  3.5 0.7 pad_maximum_fusion.1.wb_ref
  4.2 0.0 copy-done.3
  4.2 0.0 copy-start.4
  4.2 0.7 tile.21.kg_ref
  4.8 0.0 copy-done.4
  4.9 0.7 tile.9.qg_ref
  5.6 0.6 broadcast_in_dim.2.slope_ref
  6.2 80.2 %layer.1 = bf16[4,128,256]{2,1,0:T(8,128)(2,1)} custom-call(bf16[4,128,1024]{2,1,0:T(8,128)(2,1)} %x_ref.1, f32[1,1024]{1,0:T(1,128)} %bitcast.11, bf16[128,768]{1,0:T(8,128)(2,1)} %reshape.29.wa_ref, bf16[128,512]{1,0:T(8,128)(2,1)} %pad_maximum_fusion.1.wb_ref, f32[3,128]{1,0:T(4,128)} %tile.9.qg_ref, f32[3,128]{1,0:T(4,128)} %tile.21.kg_ref, ...), custom_call_target="tpu_custom_call" | custom-call | tf_op jit(solution)/shard_map/layer/pallas_call | solution.py:264
  86.4 1.7 %copy.18 = bf16[4,128,256]{2,1,0:T(8,128)(2,1)} copy(bf16[4,128,256]{2,1,0:T(8,128)(2,1)} %layer.1) | data formatting | bytes 524288
  (3 shorter events, 0.0 us)
Async XLA Ops:
  0.0 1.1 %copy-start.1 = (bf16[128,3,2,64]{0,3,2,1:T(8,128)(2,1)S(1)}, bf16[128,3,2,64]{0,3,2,1:T(8,128)(2,1)}, u32[]{:S(2)}) copy-start(bf16[128,3,2,64]{0,3,2,1:T(8,128)(2,1)} %param.12) | copy-start | bytes 294916
  1.7 0.9 %copy-start = (bf16[128,3,2,64]{0,3,2,1:T(8,128)(2,1)S(1)}, bf16[128,3,2,64]{0,3,2,1:T(8,128)(2,1)}, u32[]{:S(2)}) copy-start(bf16[128,3,2,64]{0,3,2,1:T(8,128)(2,1)} %param.10) | copy-start | bytes 294916
  2.6 0.8 copy-start.2
  3.5 0.7 copy-start.3
  4.2 0.7 copy-start.4

commit v2 on v1

--- a/solution.py
+++ b/solution.py
@@ -24,9 +24,9 @@
 
 
 def layer_kernel(
-    n, tp, batch, length, heads, width, x_ref, gain_ref, wa_ref, wb_ref, qg_ref, kg_ref, slope_ref, out_ref,
-    abuf, bbuf, win0, win1, win2, qn, bias, merged, parts, got,
-    rs_send, rs_recv, ring_send, ring_recv, halo_send, halo_recv,
+    n, tp, batch, length, heads, width, x_ref, gain_ref, wa_ref, wb_ref, qg_ref, kg_ref, out_ref,
+    abuf, bbuf, win0, win1, win2, qn, bias, sums, totals, parts, got, halves, others,
+    near_send, near_recv, rs_send, rs_recv, ring_send, ring_recv, halo_send, halo_recv,
 ):
     me = lax.axis_index("sp")
     mine = lax.axis_index("tp")
@@ -72,6 +72,10 @@
     scale = lax.rsqrt(jnp.mean(flat * flat, axis=-1, keepdims=True) + EPS)
     normed = (flat * scale * gain_ref[...]).astype(jnp.bfloat16)
 
+    slopes = []
+    for head in range(heads):
+        power = -8.0 * (mine * heads + head + 1).astype(jnp.float32) / (heads * tp)
+        slopes.append(jnp.exp2(jnp.full((8, 128), power, jnp.float32))[:1, :1])
     widths = [length + 2 * d * h for d, h in GAPS]
     starts = [sum(widths[:g]) for g in range(groups)]
     for group, (dilation, half) in enumerate(GAPS):
@@ -83,7 +87,7 @@
         allowed = (offset <= reach) & (at >= 0) & (at < n * length) & ((offset & (dilation - 1)) == 0)
         distance = offset.astype(jnp.float32) / float(reach)
         for head in range(heads):
-            value = jnp.where(allowed, -slope_ref[head : head + 1, :1] * distance, NEG)
+            value = jnp.where(allowed, -slopes[head] * distance, NEG)
             bias[head, :, starts[group] : starts[group] + widths[group]] = value
 
     wins = (win0, win1, win2)
@@ -116,6 +120,9 @@
     column_head = lax.broadcasted_iota(jnp.int32, (lanes, lanes), 1) // width
     same_head = jnp.where(row_head == column_head, 1.0 / width, 0.0)
 
+    def repeated(ref, group):
+        return jnp.concatenate([ref[group : group + 1, :]] * heads, axis=1)
+
     def head_norm(block, gain):
         values = block.astype(jnp.bfloat16).astype(jnp.float32)
         mean = jnp.dot(
@@ -129,7 +136,7 @@
     for group, (dilation, half) in enumerate(GAPS):
         reach = dilation * half
         low = 2 * lanes * group
-        keys = head_norm(key_values[:, low : low + lanes], kg_ref[group : group + 1, :])
+        keys = head_norm(key_values[:, low : low + lanes], repeated(kg_ref, group))
         values = key_values[:, low + lanes : low + 2 * lanes]
         wins[group][:, reach : reach + length, :lanes] = keys.astype(jnp.bfloat16).reshape(batch, length, lanes)
         wins[group][:, reach : reach + length, lanes:] = values.astype(jnp.bfloat16).reshape(batch, length, lanes)
@@ -156,8 +163,10 @@
             device_id_type=MESH,
         )
 
-    def each_halo(method_up, method_down, inward):
+    def each_halo(method_up, method_down, inward, only=None):
         for index, (group, distance, count) in enumerate(plan):
+            if only is not None and group != only:
+                continue
             above = me + distance < n
             below = me >= distance
 
@@ -176,67 +185,105 @@
     weights = bbuf[:, :, : groups * lanes].reshape(depth, groups * lanes)
     queries = jnp.dot(normed, weights, preferred_element_type=jnp.float32)
     for group in range(groups):
-        block = head_norm(queries[:, lanes * group : lanes * (group + 1)], qg_ref[group : group + 1, :] * factor)
+        block = head_norm(queries[:, lanes * group : lanes * (group + 1)], repeated(qg_ref, group) * factor)
         qn[group] = block.astype(jnp.bfloat16).reshape(batch, length, lanes)
 
-    each_halo(lambda c: c.wait_recv(), lambda c: c.wait_recv(), True)
-
     lane_head = lax.broadcasted_iota(jnp.int32, (length, lanes), 1) // width
-
-    def attend(b, carry):
-        result = jnp.zeros((length, lanes), jnp.float32)
+    span = depth // tp
+    pairs = tp // 2
+    parity = mine % 2
+    level = mine // 2
+
+    def attend(group, b):
+        total = jnp.zeros((length, lanes), jnp.float32)
+        summed = jnp.zeros((length, lanes), jnp.float32)
+        query_all = qn[group, b]
         for head in range(heads):
             here = lane_head == head
-            total = jnp.zeros((length, 1), jnp.float32)
-            summed = jnp.zeros((length, lanes), jnp.float32)
-            for group in range(groups):
-                query = qn[group, b]
-                query = jnp.where(here, query, jnp.zeros_like(query))
-                scores = lax.dot_general(
-                    query, wins[group][b, :, :lanes], (((1,), (1,)), ((), ())), preferred_element_type=jnp.float32
-                )
-                scores = scores + bias[head, :, starts[group] : starts[group] + widths[group]]
-                grown = jnp.exp(scores)
-                total = total + jnp.sum(grown, axis=-1, keepdims=True)
-                summed = summed + jnp.dot(
-                    grown.astype(jnp.bfloat16), wins[group][b, :, lanes:], preferred_element_type=jnp.float32
-                )
-            result = jnp.where(here, summed / total, result)
-        merged[b] = result.astype(jnp.bfloat16)
+            query = jnp.where(here, query_all, jnp.zeros_like(query_all))
+            scores = lax.dot_general(
+                query, wins[group][b, :, :lanes], (((1,), (1,)), ((), ())), preferred_element_type=jnp.float32
+            )
+            grown = jnp.exp(scores + bias[head, :, starts[group] : starts[group] + widths[group]])
+            total = jnp.where(here, jnp.sum(grown, axis=-1, keepdims=True), total)
+            result = jnp.dot(
+                grown.astype(jnp.bfloat16), wins[group][b, :, lanes:], preferred_element_type=jnp.float32
+            )
+            summed = jnp.where(here, result, summed)
+        return summed, total
+
+    def to_partner(b):
+        return pltpu.make_async_remote_copy(
+            src_ref=parts.at[b, 1 - parity],
+            dst_ref=got.at[b],
+            send_sem=near_send.at[b],
+            recv_sem=near_recv.at[b],
+            device_id={"tp": mine + 1 - 2 * parity},
+            device_id_type=MESH,
+        )
+
+    def to_level(b, shift):
+        target = (level + shift) % pairs
+        return pltpu.make_async_remote_copy(
+            src_ref=halves.at[b, target],
+            dst_ref=others.at[b, shift - 1],
+            send_sem=rs_send.at[b, shift - 1],
+            recv_sem=rs_recv.at[b, shift - 1],
+            device_id={"tp": 2 * target + parity},
+            device_id_type=MESH,
+        )
+
+    def pass_on(b):
+        to_partner(b).wait_recv()
+        halves[b] = (parts[b, parity].astype(jnp.float32) + got[b].astype(jnp.float32)).astype(jnp.bfloat16)
+        for shift in range(1, pairs):
+            to_level(b, shift).start()
+
+    outs = bbuf[:, :, groups * lanes :].reshape(depth, lanes)
+
+    def first_groups(group):
+        def step(b, carry):
+            summed, total = attend(group, b)
+            if group == 0:
+                sums[b], totals[b] = summed, total
+            else:
+                sums[b] += summed
+                totals[b] += total
+            return carry
+
+        return step
+
+    def last_group(b, carry):
+        summed, total = attend(groups - 1, b)
+        merged = ((sums[b] + summed) / (totals[b] + total)).astype(jnp.bfloat16)
+        term = lax.dot_general(merged, outs, (((1,), (1,)), ((), ())), preferred_element_type=jnp.float32)
+        for block in range(tp):
+            parts[b, block % 2, block // 2] = term[:, block * span : (block + 1) * span].astype(jnp.bfloat16)
+        to_partner(b).start()
+
+        @pl.when(b >= 1)
+        def _():
+            pass_on(b - 1)
+
         return carry
 
-    lax.fori_loop(0, batch, attend, 0)
-
-    both = merged[...].reshape(rows, lanes)
-    outs = bbuf[:, :, groups * lanes :].reshape(depth, lanes)
-    span = depth // tp
-    for block in range(tp):
-        term = lax.dot_general(
-            both, outs[block * span : (block + 1) * span], (((1,), (1,)), ((), ())), preferred_element_type=jnp.float32
-        )
-        parts[block] = term.astype(jnp.bfloat16)
-
-    def exchange(shift):
-        target = (mine + shift) % tp
-        return pltpu.make_async_remote_copy(
-            src_ref=parts.at[target],
-            dst_ref=got.at[shift - 1],
-            send_sem=rs_send.at[shift - 1],
-            recv_sem=rs_recv.at[shift - 1],
-            device_id={"tp": target},
-            device_id_type=MESH,
-        )
-
-    for shift in range(1, tp):
-        exchange(shift).start()
-    summed = parts[mine].astype(jnp.float32)
-    for shift in range(1, tp):
-        exchange(shift).wait_recv()
-        summed = summed + got[shift - 1].astype(jnp.float32)
-    out_ref[...] = summed.astype(jnp.bfloat16).reshape(batch, length, span)
-
-    for shift in range(1, tp):
-        exchange(shift).wait_send()
+    for group in range(groups):
+        each_halo(lambda c: c.wait_recv(), lambda c: c.wait_recv(), True, group)
+        lax.fori_loop(0, batch, last_group if group == groups - 1 else first_groups(group), 0)
+    pass_on(batch - 1)
+
+    def finish(b, carry):
+        final = parts[b, parity, level].astype(jnp.float32) + got[b, level].astype(jnp.float32)
+        for shift in range(1, pairs):
+            to_level(b, shift).wait_recv()
+            final = final + others[b, shift - 1].astype(jnp.float32)
+        out_ref[b] = final.astype(jnp.bfloat16)
+        for shift in range(1, pairs):
+            to_level(b, shift).wait_send()
+        to_partner(b).wait_send()
+        return carry
+
+    lax.fori_loop(0, batch, finish, 0)
     for step in range(1, half_n + 1):
         for chunk in range(2):
             for way in range(2):
@@ -253,9 +300,6 @@
     ).reshape(share, groups * 2 * lanes)
     outs = out_weight.reshape(lanes, -1).T
     rest = jnp.concatenate([query_weight.reshape(share, groups * lanes), outs], axis=1)
-    index = lax.axis_index("tp") * heads + jnp.arange(heads)
-    slopes = jnp.exp2(-8.0 * (index + 1).astype(jnp.float32) / (heads * tp))
-    slopes = jnp.broadcast_to(slopes[:, None], (heads, 128))
     total = sum(length + 2 * d * h for d, h in GAPS)
     windows = [pltpu.VMEM((batch, length + 2 * d * h, 2 * lanes), jnp.bfloat16) for d, h in GAPS]
     plan = halo_plan(length)
@@ -264,7 +308,7 @@
     return pl.pallas_call(
         functools.partial(layer_kernel, n, tp, batch, length, heads, width),
         out_shape=jax.ShapeDtypeStruct((batch, length, span), jnp.bfloat16),
-        in_specs=[vmem] * 7,
+        in_specs=[vmem] * 6,
         out_specs=vmem,
         scratch_shapes=[
             pltpu.VMEM((n, share, key_values.shape[1]), jnp.bfloat16),
@@ -272,11 +316,16 @@
             *windows,
             pltpu.VMEM((groups, batch, length, lanes), jnp.bfloat16),
             pltpu.VMEM((heads, length, total), jnp.float32),
-            pltpu.VMEM((batch, length, lanes), jnp.bfloat16),
-            pltpu.VMEM((tp, batch * length, span), jnp.bfloat16),
-            pltpu.VMEM((tp - 1, batch * length, span), jnp.bfloat16),
-            pltpu.SemaphoreType.DMA((tp - 1,)),
-            pltpu.SemaphoreType.DMA((tp - 1,)),
+            pltpu.VMEM((batch, length, lanes), jnp.float32),
+            pltpu.VMEM((batch, length, lanes), jnp.float32),
+            pltpu.VMEM((batch, 2, tp // 2, length, span), jnp.bfloat16),
+            pltpu.VMEM((batch, tp // 2, length, span), jnp.bfloat16),
+            pltpu.VMEM((batch, tp // 2, length, span), jnp.bfloat16),
+            pltpu.VMEM((batch, tp // 2 - 1, length, span), jnp.bfloat16),
+            pltpu.SemaphoreType.DMA((batch,)),
+            pltpu.SemaphoreType.DMA((batch,)),
+            pltpu.SemaphoreType.DMA((batch, tp // 2 - 1)),
+            pltpu.SemaphoreType.DMA((batch, tp // 2 - 1)),
             pltpu.SemaphoreType.DMA((2, 2, n // 2)),
             pltpu.SemaphoreType.DMA((2, 2, n // 2)),
             pltpu.SemaphoreType.DMA((2, len(plan))),
@@ -289,9 +338,8 @@
         norm_gain.reshape(1, model),
         key_values,
         rest,
-        jnp.tile(query_gain, (1, heads)),
-        jnp.tile(key_gain, (1, heads)),
-        slopes,
+        query_gain,
+        key_gain,
     )
 
 

time: 88.4 us -> 79 us (0.89)
  Pallas kernels: 80.2 us -> 72.9 us
  local copies, waits for them, and re-layouts: 6.66 us -> 4.66 us
    pallas_call x1, Pallas kernels: 80.2 us -> 72.9 us  [body(): pl.pallas_call(functools.partial(layer_kernel, n, tp, batch, length, head...]
    another operation x4 -> x0, local copies, waits for them, and re-layouts: 1.34 us -> none  [the longest x2 0.68 us: body(): jnp.tile(query_gain, (1, heads))]
    unnamed x11 -> x7, local copies, waits for them, and re-layouts: 2.47 us -> 2.42 us
where the time goes in v2:
time: 79 us; the launch traced here: 78.7 us
  Pallas kernels  72.9 us (92%)
  local copies, waits for them, and re-layouts  4.66 us (6%)
  other arithmetic  1.15 us (1%)
    pallas_call x1, Pallas kernels, body(): pl.pallas_call(functools.partial(layer_kernel, n, tp, batch, length, head...  72.9 us
    unnamed x7, local copies, waits for them, and re-layouts  2.42 us

profile of v2, /device:TPU:17, one launch (start us, length us, event | category | flops | bytes accessed | tf_op | source)
XLA Modules:
  0.0 78.7 jit_solution(12524479541605564623)
XLA Ops:
  0.0 0.0 copy-start.1
  0.0 1.1 %copy.13 = bf16[128,3,1,128]{3,2,1,0:T(2,128)(2,1)S(1)} copy(bf16[128,3,1,128]{0,3,1,2:T(8,128)(2,1)} %bitcast.8) | data formatting | bytes 196608 | tf_op jit(solution)/shard_map/stack;reshape | solution.py:298
  1.1 0.0 copy-done.1
  1.1 0.2 copy.14
  1.3 0.5 pad_maximum_fusion
  1.7 0.0 copy-start
  1.7 0.8 reshape.13.wa_ref
  2.5 0.1 copy-done
  2.6 0.0 copy-start.2
  2.6 0.1 copy.16
  2.7 0.6 copy-done.2
  3.4 0.1 copy.15
  3.5 0.7 pad_maximum_fusion.1.wb_ref
  4.2 72.9 %layer.1 = bf16[4,128,256]{2,1,0:T(8,128)(2,1)} custom-call(bf16[4,128,1024]{2,1,0:T(8,128)(2,1)} %x_ref.1, f32[1,1024]{1,0:T(1,128)} %bitcast.11, bf16[128,768]{1,0:T(8,128)(2,1)} %reshape.13.wa_ref, bf16[128,512]{1,0:T(8,128)(2,1)} %pad_maximum_fusion.1.wb_ref, f32[3,64]{1,0:T(4,128)} %qg_ref.1, f32[3,64]{1,0:T(4,128)} %kg_ref.1), custom_call_target="tpu_custom_call" | custom-call | tf_op jit(solution)/shard_map/layer/pallas_call | solution.py:308
  77.1 1.7 %copy.18 = bf16[4,128,256]{2,1,0:T(8,128)(2,1)} copy(bf16[4,128,256]{2,1,0:T(8,128)(2,1)} %layer.1) | data formatting | bytes 524288
Async XLA Ops:
  0.0 1.1 %copy-start.1 = (bf16[128,3,2,64]{0,3,2,1:T(8,128)(2,1)S(1)}, bf16[128,3,2,64]{0,3,2,1:T(8,128)(2,1)}, u32[]{:S(2)}) copy-start(bf16[128,3,2,64]{0,3,2,1:T(8,128)(2,1)} %param.12) | copy-start | bytes 294916
  1.7 0.9 %copy-start = (bf16[128,3,2,64]{0,3,2,1:T(8,128)(2,1)S(1)}, bf16[128,3,2,64]{0,3,2,1:T(8,128)(2,1)}, u32[]{:S(2)}) copy-start(bf16[128,3,2,64]{0,3,2,1:T(8,128)(2,1)} %param.10) | copy-start | bytes 294916
  2.6 0.8 copy-start.2

commit v3 on v2

--- a/solution.py
+++ b/solution.py
@@ -61,6 +61,32 @@
             device_id={"sp": forward if way == 0 else backward},
             device_id_type=MESH,
         )
+
+    barrier = pltpu.get_barrier_semaphore()
+
+    def greet(target):
+        pl.semaphore_signal(barrier, inc=1, device_id=target, device_id_type=MESH)
+
+    greet({"sp": forward})
+    greet({"sp": backward})
+    greet({"tp": mine + 1 - 2 * (mine % 2)})
+    for shift in range(1, tp // 2):
+        greet({"tp": (mine + 2 * shift) % tp})
+    plan = halo_plan(length)
+    for distance in sorted({item[1] for item in plan}):
+
+        @pl.when(me + distance < n)
+        def _(distance=distance):
+            greet({"sp": me + distance})
+
+        @pl.when(me >= distance)
+        def _(distance=distance):
+            greet({"sp": me - distance})
+
+    count = 2 + tp // 2
+    for distance in sorted({item[1] for item in plan}):
+        count = count + jnp.where(me + distance < n, 1, 0) + jnp.where(me >= distance, 1, 0)
+    pl.semaphore_wait(barrier, count)
 
     for chunk in range(2):
         for way in range(2):
@@ -91,7 +117,6 @@
             bias[head, :, starts[group] : starts[group] + widths[group]] = value
 
     wins = (win0, win1, win2)
-    plan = halo_plan(length)
     for group, distance, count in plan:
         reach = GAPS[group][0] * GAPS[group][1]
         low = reach - (distance - 1) * length - count
@@ -110,11 +135,15 @@
         for way in range(2):
             hop(chunk, way, half_n).wait_recv()
 
-    for step in range(2, half_n + 1):
-        for chunk in range(2):
+    def advance(chunk, step):
+        if 2 <= step <= half_n:
             for way in range(2):
                 hop(chunk, way, step - 1).wait_recv()
                 hop(chunk, way, step).start()
+
+    for step in range(2, half_n + 1):
+        advance(0, step)
+        advance(1, step - 1)
 
     row_head = lax.broadcasted_iota(jnp.int32, (lanes, lanes), 0) // width
     column_head = lax.broadcasted_iota(jnp.int32, (lanes, lanes), 1) // width
@@ -132,15 +161,6 @@
 
     finish_ring(0)
     depth = abuf.shape[0] * abuf.shape[1]
-    key_values = jnp.dot(normed, abuf[...].reshape(depth, -1), preferred_element_type=jnp.float32)
-    for group, (dilation, half) in enumerate(GAPS):
-        reach = dilation * half
-        low = 2 * lanes * group
-        keys = head_norm(key_values[:, low : low + lanes], repeated(kg_ref, group))
-        values = key_values[:, low + lanes : low + 2 * lanes]
-        wins[group][:, reach : reach + length, :lanes] = keys.astype(jnp.bfloat16).reshape(batch, length, lanes)
-        wins[group][:, reach : reach + length, lanes:] = values.astype(jnp.bfloat16).reshape(batch, length, lanes)
-
     def halo(index, up):
         group, distance, count = plan[index]
         reach = GAPS[group][0] * GAPS[group][1]
@@ -178,7 +198,18 @@
             def _(index=index):
                 method_down(halo(index, False))
 
-    each_halo(lambda c: c.start(), lambda c: c.start(), False)
+    for group in reversed(range(groups)):
+        reach = GAPS[group][0] * GAPS[group][1]
+        low = 2 * lanes * group
+        weights = abuf[:, :, low : low + 2 * lanes].reshape(depth, 2 * lanes)
+        key_values = jnp.dot(normed, weights, preferred_element_type=jnp.float32)
+        keys = head_norm(key_values[:, :lanes], repeated(kg_ref, group))
+        values = key_values[:, lanes:]
+        wins[group][:, reach : reach + length, :lanes] = keys.astype(jnp.bfloat16).reshape(batch, length, lanes)
+        wins[group][:, reach : reach + length, lanes:] = values.astype(jnp.bfloat16).reshape(batch, length, lanes)
+        if group == groups - 1:
+            advance(1, half_n)
+        each_halo(lambda c: c.start(), lambda c: c.start(), False, group)
 
     finish_ring(1)
     factor = 1.0 / math.sqrt(width)
@@ -244,7 +275,7 @@
     def first_groups(group):
         def step(b, carry):
             summed, total = attend(group, b)
-            if group == 0:
+            if group == groups - 1:
                 sums[b], totals[b] = summed, total
             else:
                 sums[b] += summed
@@ -254,7 +285,7 @@
         return step
 
     def last_group(b, carry):
-        summed, total = attend(groups - 1, b)
+        summed, total = attend(0, b)
         merged = ((sums[b] + summed) / (totals[b] + total)).astype(jnp.bfloat16)
         term = lax.dot_general(merged, outs, (((1,), (1,)), ((), ())), preferred_element_type=jnp.float32)
         for block in range(tp):
@@ -267,9 +298,9 @@
 
         return carry
 
-    for group in range(groups):
+    for group in reversed(range(groups)):
         each_halo(lambda c: c.wait_recv(), lambda c: c.wait_recv(), True, group)
-        lax.fori_loop(0, batch, last_group if group == groups - 1 else first_groups(group), 0)
+        lax.fori_loop(0, batch, last_group if group == 0 else first_groups(group), 0)
     pass_on(batch - 1)
 
     def finish(b, carry):
@@ -331,7 +362,7 @@
             pltpu.SemaphoreType.DMA((2, len(plan))),
             pltpu.SemaphoreType.DMA((2, len(plan))),
         ],
-        compiler_params=pltpu.CompilerParams(has_side_effects=True, vmem_limit_bytes=60 * 1024 * 1024),
+        compiler_params=pltpu.CompilerParams(collective_id=0, has_side_effects=True, vmem_limit_bytes=60 * 1024 * 1024),
         name="layer",
     )(
         inputs,

time: 79 us -> 74.9 us (0.948); the launches traced: 78.7 us -> 73.5 us
  Pallas kernels: 72.9 us -> 67.6 us
    pallas_call x1, Pallas kernels: 72.9 us -> 67.6 us  [body(): pl.pallas_call(functools.partial(layer_kernel, n, tp, batch, length, head...]
where the time goes in v3:
time: 74.9 us; the launch traced here: 73.5 us
  Pallas kernels  67.6 us (90%)
  local copies, waits for them, and re-layouts  4.66 us (6%)
  other arithmetic  1.15 us (2%)
    pallas_call x1, Pallas kernels, body(): pl.pallas_call(functools.partial(layer_kernel, n, tp, batch, length, head...  67.6 us
    unnamed x7, local copies, waits for them, and re-layouts  2.42 us

profile of v3, /device:TPU:17, one launch (start us, length us, event | category | flops | bytes accessed | tf_op | source)
XLA Modules:
  0.0 73.5 jit_solution(12393737770428301957)
XLA Ops:
  0.0 0.0 copy-start.1
  0.0 1.1 %copy.13 = bf16[128,3,1,128]{3,2,1,0:T(2,128)(2,1)S(1)} copy(bf16[128,3,1,128]{0,3,1,2:T(8,128)(2,1)} %bitcast.8) | data formatting | bytes 196608 | tf_op jit(solution)/shard_map/stack;reshape | solution.py:329
  1.1 0.0 copy-done.1
  1.1 0.2 copy.14
  1.3 0.5 pad_maximum_fusion
  1.7 0.0 copy-start
  1.7 0.8 %reshape.13.wa_ref = bf16[128,768]{1,0:T(8,128)(2,1)} reshape(bf16[128,3,2,128]{3,2,1,0:T(2,128)(2,1)S(1)} %pad_maximum_fusion) | data formatting | bytes 393216 | tf_op jit(solution)/shard_map/reshape | solution.py:331
  2.5 0.1 copy-done
  2.6 0.0 copy-start.2
  2.6 0.1 copy.16
  2.7 0.6 copy-done.2
  3.4 0.1 copy.15
  3.5 0.7 pad_maximum_fusion.1.wb_ref
  4.2 67.6 %layer.1 = bf16[4,128,256]{2,1,0:T(8,128)(2,1)} custom-call(bf16[4,128,1024]{2,1,0:T(8,128)(2,1)} %x_ref.1, f32[1,1024]{1,0:T(1,128)} %bitcast.11, bf16[128,768]{1,0:T(8,128)(2,1)} %reshape.13.wa_ref, bf16[128,512]{1,0:T(8,128)(2,1)} %pad_maximum_fusion.1.wb_ref, f32[3,64]{1,0:T(4,128)} %qg_ref.1, f32[3,64]{1,0:T(4,128)} %kg_ref.1), custom_call_target="tpu_custom_call" | custom-call | tf_op jit(solution)/shard_map/layer/pallas_call | solution.py:339
  71.8 1.7 %copy.18 = bf16[4,128,256]{2,1,0:T(8,128)(2,1)} copy(bf16[4,128,256]{2,1,0:T(8,128)(2,1)} %layer.1) | data formatting | bytes 524288
Async XLA Ops:
  0.0 1.1 %copy-start.1 = (bf16[128,3,2,64]{0,3,2,1:T(8,128)(2,1)S(1)}, bf16[128,3,2,64]{0,3,2,1:T(8,128)(2,1)}, u32[]{:S(2)}) copy-start(bf16[128,3,2,64]{0,3,2,1:T(8,128)(2,1)} %param.12) | copy-start | bytes 294916
  1.7 0.9 %copy-start = (bf16[128,3,2,64]{0,3,2,1:T(8,128)(2,1)S(1)}, bf16[128,3,2,64]{0,3,2,1:T(8,128)(2,1)}, u32[]{:S(2)}) copy-start(bf16[128,3,2,64]{0,3,2,1:T(8,128)(2,1)} %param.10) | copy-start | bytes 294916
  2.6 0.8 %copy-start.2 = (bf16[2,64,128]{2,1,0:T(8,128)(2,1)S(1)}, bf16[2,64,128]{2,1,0:T(8,128)(2,1)}, u32[]{:S(2)}) copy-start(bf16[2,64,128]{2,1,0:T(8,128)(2,1)} %param.15) | copy-start | bytes 98308
